TPU v7x, 256 devices: a whole 4x4x8 slice. The times are simulated.
256 devices in a mesh: sp: 32 (over z, x), fs: 4 (over y), tp: 2 (over core).
Axes of the slice: x: 4, y: 4, z: 8, core: 2. Of those that a mesh axis runs over, the one named last changes fastest.
Arguments:
- inputs: bfloat16 [4, 4096, 2048], P('fs', 'sp'), may hold values from -6 to 6
- input_norm_gain: bfloat16 [2048], replicated, may hold values from 0.099609375 to 1.8984375
- receptance_matrix: bfloat16 [2048, 1024], P('fs', 'tp'), may hold values from -0.125 to 0.125
- key_matrix: bfloat16 [2048, 1024], P('fs', 'tp'), may hold values from -0.125 to 0.125
- value_matrix: bfloat16 [2048, 1024], P('fs', 'tp'), may hold values from -0.125 to 0.125
- pooling_input_weight: bfloat16 [2048, 1024], P('fs', 'tp'), may hold values from -0.125 to 0.125
- decay_lower_matrix: bfloat16 [2048, 128], replicated, may hold values from -0.125 to 0.125
- decay_raise_matrix: bfloat16 [2, 64, 1024], P(None, None, 'tp'), may hold values from -1 to 1
- decay_offset_bias: float32 [2, 1024], P(None, 'tp'), may hold values from -13 to -3
- removal_lower_matrix: bfloat16 [2048, 128], replicated, may hold values from -0.125 to 0.125
- removal_raise_matrix: bfloat16 [2, 64, 1024], P(None, None, 'tp'), may hold values from -1 to 1
- removal_rate_bias: float32 [2, 1024], P(None, 'tp'), may hold values from -9 to 1.5
- tempo_scale: float32 [4, 2, 16, 4096], P('fs', None, 'tp', 'sp'), may hold values from 0.3 to 3.2, as said below
- sudden_decay_extra: float32 [4, 2, 16, 4096], P('fs', None, 'tp', 'sp'), may hold values from -2.8 to 0
- head_norm_gain: bfloat16 [1024], P('tp'), may hold values from 0.099609375 to 1.8984375
- group_mixing_weight: bfloat16 [4, 256, 256], P('tp'), may hold values from -0.375 to 0.375
- attention_output_matrix: bfloat16 [2048, 1024], P('fs', 'tp'), may hold values from -0.125 to 0.125
- pooling_output_matrix: bfloat16 [2048, 1024], P('fs', 'tp'), may hold values from -0.125 to 0.125
Outputs:
- mixed_out: bfloat16 [4, 4096, 2048], P('fs', ('sp', 'tp'))
Inputs may be any that keep to these rules, and one draw needn't show every extreme that they name: `tempo_scale`: positive.
All inputs are finite; a program needn't handle non-finite values.
Results may differ from a plain program's by a relative error of at most 0.017.
Values may be sent and summed in bfloat16 or wider, within the bound.
No kernel may reach another device: no remote copies, remote signals or barrier semaphores. Data moves between devices by JAX's collectives and lax.ppermute only.
A program may use at most 128 MiB of HBM per device.

v0:
```python
import jax
import jax.numpy as jnp
from jax import lax
from jax.sharding import Mesh
from jax.sharding import PartitionSpec as P

HEAD = 64
DECAY_RANK = 64
RATE_RANK = 64
POOL_GROUPS = 4
GROUP_WIDTH = 256
SP = ("sp_0", "sp_1")
SP_TP = ("sp_0", "sp_1", "tp")
norm_eps = 1e-06
head_eps = 0.00064
unit_eps = 1e-06
span_len = 32
highest = lax.Precision.HIGHEST


def filled_with(shard, identity):
    return jax.tree.map(
        lambda a, e: jnp.broadcast_to(jnp.asarray(e, a.dtype), a.shape), shard, identity
    )


def prefix_by_axis(shard, axes, combine, identity, reverse):
    before = start = filled_with(shard, identity)
    total = shard
    for axis in reversed(axes):
        peers, here = (lax.axis_size(axis), lax.axis_index(axis))
        pieces = jax.tree.map(
            lambda part, kind: lax.all_gather(part.astype(kind), axis),
            total,
            (jnp.bfloat16, jnp.bfloat16),
        )
        inside, total = (start, start)
        for k in reversed(range(peers)) if reverse else range(peers):
            passed = k > here if reverse else k < here
            total = combine(
                total, jax.tree.map(lambda part, own: part[k].astype(own.dtype), pieces, shard)
            )
            inside = jax.tree.map(lambda new, old: jnp.where(passed, new, old), total, inside)
        before = combine(inside, before)
    return before


def with_halo(cells, sides, width):
    for axis, dim in sides:
        count = lax.axis_size(axis)
        ends = count - 1
        head = lax.slice_in_dim(cells, 0, width, axis=dim)
        tail = lax.slice_in_dim(cells, cells.shape[dim] - width, cells.shape[dim], axis=dim)
        cells = jnp.concatenate(
            [
                lax.ppermute(tail, axis, [(i, (i + 1) % count) for i in range(ends)]),
                cells,
                lax.ppermute(head, axis, [((i + 1) % count, i) for i in range(ends)]),
            ],
            axis=dim,
        )
    return cells


def contract(form, left, right):
    return jnp.einsum(form, left, right, precision=highest)


def matmul(left, right):
    return contract("...ij,...jk->...ik", left, right)


def project(left, weight):
    return jnp.dot(left, weight, preferred_element_type=jnp.float32).astype(jnp.bfloat16)


def against(row_block, weight):
    return lax.dot_general(
        row_block, weight, (((1,), (1,)), ((), ())), preferred_element_type=jnp.float32
    )


def chain_combine(earlier, later):
    return (matmul(earlier[0], later[0]), matmul(earlier[1], later[0]) + later[1])


def unit_inverse(lower):
    result = jnp.eye(lower.shape[-1], dtype=jnp.float32) - lower
    power = lower
    for level in range(4):
        power = matmul(power, power)
        result = result + matmul(result, power)
    return result


def span_terms(logarithm_decay, unit, removal, written, value, recept):
    inner = jnp.cumsum(logarithm_decay, axis=-2)
    last = inner[..., -1:, :]
    ahead = unit * jnp.exp(inner - logarithm_decay)
    shrink = jnp.exp(-inner)
    remove_scaled = removal * shrink
    write_scaled = written * shrink
    query = recept * jnp.exp(inner)
    spots = jnp.arange(span_len)
    strict = spots[:, None] > spots[None, :]
    within = spots[:, None] >= spots[None, :]
    link_remove = jnp.where(strict, contract("...tk,...sk->...ts", ahead, remove_scaled), 0.0)
    link_write = jnp.where(strict, contract("...tk,...sk->...ts", ahead, write_scaled), 0.0)
    read_remove = jnp.where(within, contract("...tk,...sk->...ts", query, remove_scaled), 0.0)
    read_write = jnp.where(within, contract("...tk,...sk->...ts", query, write_scaled), 0.0)
    inverse = unit_inverse(link_remove)
    pull_map = -matmul(inverse, ahead)
    pull_base = -matmul(inverse, matmul(link_write, value))
    tail = jnp.exp(last - inner)
    remove_tail = removal * tail
    write_tail = written * tail
    transfer = jnp.eye(unit.shape[-1], dtype=jnp.float32) * jnp.exp(last) + contract(
        "...sk,...sj->...kj", pull_map, remove_tail
    )
    carried = contract("...sv,...sk->...vk", pull_base, remove_tail) + contract(
        "...sv,...sk->...vk", value, write_tail
    )
    query_eff = query + matmul(read_remove, pull_map)
    local_read = matmul(read_remove, pull_base) + matmul(read_write, value)
    return (query_eff, local_read, transfer, carried)


def shards(
    inputs,
    input_norm_gain,
    receptance_matrix,
    key_matrix,
    value_matrix,
    pooling_input_weight,
    decay_lower_matrix,
    decay_raise_matrix,
    decay_offset_bias,
    removal_lower_matrix,
    removal_raise_matrix,
    removal_rate_bias,
    tempo_scale,
    sudden_decay_extra,
    head_norm_gain,
    group_mixing_weight,
    attention_output_matrix,
    pooling_output_matrix,
):
    recept_full, key_full, value_full, pool_full, attn_full, pool_back = (
        lax.all_gather(receptance_matrix, "fs", axis=0, tiled=True),
        lax.all_gather(key_matrix, "fs", axis=0, tiled=True),
        lax.all_gather(value_matrix, "fs", axis=0, tiled=True),
        lax.all_gather(pooling_input_weight, "fs", axis=0, tiled=True),
        lax.all_gather(attention_output_matrix, "fs", axis=0, tiled=True),
        lax.all_gather(pooling_output_matrix, "fs", axis=0, tiled=True),
    )
    row_block = inputs[0].astype(jnp.float32)
    normed = (
        row_block
        * lax.rsqrt(jnp.mean(row_block * row_block, axis=-1, keepdims=True) + norm_eps)
        * input_norm_gain.astype(jnp.float32)
    ).astype(jnp.bfloat16)
    tokens = normed.shape[0]
    heads = recept_full.shape[1] // HEAD
    blocks = tokens // span_len
    receptance = project(normed, recept_full).astype(jnp.float32).reshape(tokens, heads, HEAD)
    key_rows = project(normed, key_full).astype(jnp.float32).reshape(tokens, heads, HEAD)
    val_rows = project(normed, value_full).astype(jnp.float32).reshape(tokens, heads, HEAD)
    pool_in = project(normed, pool_full)
    decay_act = jnp.tanh(project(normed, decay_lower_matrix).astype(jnp.float32)).astype(
        jnp.bfloat16
    )
    rate_latent = project(normed, removal_lower_matrix)
    unit_keys = key_rows * lax.rsqrt(
        jnp.sum(key_rows * key_rows, axis=-1, keepdims=True) + unit_eps
    )
    decays = []
    removals = []
    writes = []
    for travel_direction in range(2):
        part = decay_act[:, travel_direction * DECAY_RANK : (travel_direction + 1) * DECAY_RANK]
        decay_pre = decay_offset_bias[travel_direction] + jnp.dot(
            part, decay_raise_matrix[travel_direction], preferred_element_type=jnp.float32
        )
        decay_velocity = jnp.exp(-jax.nn.softplus(-decay_pre) - 0.5).reshape(tokens, heads, HEAD)
        decays.append(
            -decay_velocity * tempo_scale[0, travel_direction].T[:, :, None]
            + sudden_decay_extra[0, travel_direction].T[:, :, None]
        )
        latent = rate_latent[:, travel_direction * RATE_RANK : (travel_direction + 1) * RATE_RANK]
        rate = jax.nn.sigmoid(
            removal_rate_bias[travel_direction]
            + jnp.dot(
                latent, removal_raise_matrix[travel_direction], preferred_element_type=jnp.float32
            )
        )
        rate = rate.reshape(tokens, heads, HEAD)
        removals.append(unit_keys * rate)
        writes.append(key_rows * rate)

    def both_ways(forward, backward):
        stacked = jnp.stack([forward, jnp.flip(backward, axis=0)], axis=0)
        return stacked.reshape(2, blocks, span_len, heads, HEAD).transpose(0, 3, 1, 2, 4)

    query_eff, local_read, transfer, carried = span_terms(
        both_ways(decays[0], decays[1]),
        both_ways(unit_keys, unit_keys),
        both_ways(removals[0], removals[1]),
        both_ways(writes[0], writes[1]),
        both_ways(val_rows, val_rows),
        both_ways(receptance, receptance),
    )
    prefix_map, prefix_sum = lax.associative_scan(chain_combine, (transfer, carried), axis=2)
    total_map = prefix_map[:, :, -1]
    total_sum = prefix_sum[:, :, -1]
    identity_map = jnp.broadcast_to(jnp.eye(HEAD, dtype=jnp.float32), total_map.shape[1:])
    empty = jnp.zeros(total_map.shape[1:], jnp.float32)
    ahead_in = prefix_by_axis(
        (total_map[0], total_sum[0]), SP, chain_combine, (identity_map, empty), False
    )
    behind_in = prefix_by_axis(
        (total_map[1], total_sum[1]), SP, chain_combine, (identity_map, empty), True
    )
    incoming = jnp.stack([ahead_in[1], behind_in[1]], axis=0)
    ending = matmul(incoming[:, :, None], prefix_map) + prefix_sum
    starting = jnp.concatenate([incoming[:, :, None], ending[:, :, :-1]], axis=2)
    reads = contract("...tk,...vk->...tv", query_eff, starting) + local_read
    reads = reads.transpose(0, 2, 3, 1, 4).reshape(2, tokens, heads, HEAD)
    readout = reads[0] + jnp.flip(reads[1], axis=0)
    centred = readout - jnp.mean(readout, axis=-1, keepdims=True)
    spread = jnp.mean(centred * centred, axis=-1, keepdims=True)
    attn_out = (centred * lax.rsqrt(spread + head_eps)).reshape(
        tokens, heads * HEAD
    ) * head_norm_gain.astype(jnp.float32)
    attn_out = attn_out.astype(jnp.bfloat16)
    reach = 2 ** (POOL_GROUPS - 1)
    rimmed = with_halo(pool_in, ((SP, 0),), reach).astype(jnp.float32)
    position = lax.axis_index(SP) * tokens + jnp.arange(tokens)
    length = tokens * lax.axis_size(SP)
    running = rimmed
    window_sums = []
    window_counts = []
    for level in range(POOL_GROUPS):
        shift = 2**level
        running = running[:-shift] + running[shift:]
        window_sums.append(running[reach - shift : reach - shift + tokens])
        upper = jnp.minimum(position + shift, length)
        lower = jnp.maximum(position - shift, 0)
        window_counts.append((upper - lower).astype(jnp.float32))
    window_sums = jnp.stack(window_sums, axis=0)
    window_counts = jnp.stack(window_counts, axis=0)
    pool_vals = pool_in.astype(jnp.float32)
    groups_here = pool_in.shape[1] // GROUP_WIDTH
    diffs = []
    for member in range(groups_here):
        group = lax.axis_index("tp") * groups_here + member
        chosen = lax.dynamic_index_in_dim(
            window_sums[:, :, member * GROUP_WIDTH : (member + 1) * GROUP_WIDTH],
            group,
            0,
            keepdims=False,
        )
        count = lax.dynamic_index_in_dim(window_counts, group, 0, keepdims=False)
        diffs.append(
            chosen / count[:, None]
            - pool_vals[:, member * GROUP_WIDTH : (member + 1) * GROUP_WIDTH]
        )
    pool_diff = jnp.concatenate(diffs, axis=1).astype(jnp.bfloat16)
    mixed = [
        jnp.dot(
            pool_diff[:, member * GROUP_WIDTH : (member + 1) * GROUP_WIDTH],
            group_mixing_weight[member],
            preferred_element_type=jnp.float32,
        )
        for member in range(groups_here)
    ]
    pool_out = jnp.concatenate(mixed, axis=1).astype(jnp.bfloat16)
    attn_half, pool_half = (
        lax.all_to_all(attn_out, "tp", split_axis=0, concat_axis=1, tiled=True),
        lax.all_to_all(pool_out, "tp", split_axis=0, concat_axis=1, tiled=True),
    )
    attn_whole, pool_whole = (
        lax.all_gather(attn_full, "tp", axis=1, tiled=True),
        lax.all_gather(pool_back, "tp", axis=1, tiled=True),
    )
    result = against(attn_half, attn_whole) + against(pool_half, pool_whole)
    return result.astype(jnp.bfloat16)[None]


def solution(mesh):
    split = Mesh(
        mesh.devices.reshape(8, 4, mesh.shape["fs"], mesh.shape["tp"]), ("sp_0", "sp_1", "fs", "tp")
    )
    in_specs = (
        P("fs", SP, None),
        P(),
        P("fs", "tp"),
        P("fs", "tp"),
        P("fs", "tp"),
        P("fs", "tp"),
        P(),
        P(None, None, "tp"),
        P(None, "tp"),
        P(),
        P(None, None, "tp"),
        P(None, "tp"),
        P("fs", None, "tp", SP),
        P("fs", None, "tp", SP),
        P("tp"),
        P("tp", None, None),
        P("fs", "tp"),
        P("fs", "tp"),
    )
    out_specs = P("fs", SP_TP, None)
    return jax.shard_map(
        shards, mesh=split, in_specs=in_specs, out_specs=out_specs, check_vma=False
    )
```

profile of v0, /device:TPU:7, one launch (start us, length us, event | category | flops | bytes accessed | tf_op | source)
XLA Modules:
  0.0 448.1 jit_solution(15655499817770157762)
XLA Ops:
  18.1 27.2 %all-gather.19.cloned.1.call-done = bf16[2048,512]{1,0:T(8,128)(2,1)} async-done(((bf16[512,512]{1,0:T(8,128)(2,1)}), bf16[2048,512]{1,0:T(8,128)(2,1)}) %all-gather.19.cloned.1.call-update) | async-done | bytes 2097168 | tf_op jit(solution)/shard_map/all_gather | solution.py:150
  45.3 2.1 fusion.29
  47.6 32.9 %all-gather.21.cloned.1.call-done = bf16[2048,512]{1,0:T(8,128)(2,1)} async-done(((bf16[512,512]{1,0:T(8,128)(2,1)}), bf16[2048,512]{1,0:T(8,128)(2,1)}) %all-gather.21.cloned.1.call-update) | async-done | bytes 2097168 | tf_op jit(solution)/shard_map/all_gather | solution.py:151
  80.5 2.1 fusion.28
  90.6 3.0 fusion.55
  93.6 3.0 convolution_select_fusion.2
  96.6 1.2 fusion.215
  97.8 1.2 fusion.216
  99.0 1.3 convolution_add_fusion.5
  100.3 1.2 fusion.217
  101.5 1.4 convolution_add_fusion.4
  102.9 2.2 fusion.218
  105.1 2.2 convolution_add_fusion.3
  107.3 4.0 convolution_select_fusion.1
  113.4 1.1 copy.129
  114.5 3.2 convolution_add_fusion.2
  117.8 1.8 convolution_negate_fusion.1
  119.6 1.2 fusion.61
  120.8 1.2 convolution_negate_fusion
  122.0 4.2 fusion.46
  126.3 5.0 %multiply_add_fusion = f32[2,8,4,64,64]{4,3,2,1,0:T(8,128)S(1)} fusion(f32[2,8,4,32,64]{4,3,2,1,0:T(8,128)S(1)} %convolution_negate_fusion.1, f32[2,8,4,64]{3,2,1,0:T(4,128)S(1)} %copy-done.59, f32[64,64]{1,0:T(8,128)S(1)} %fusion.167, f32[2,8,4,32,64]{4,1,2,3,0:T(8,128)} %copy-done.15), kind=kOutput, calls=%fused_computation.8 | convolution fusion | flops 101187584 | bytes 2129920 | tf_op jit(solution)/shard_map/...sk,...sj->...kj/dot_general | solution.py:66
  131.3 1.2 fusion.41
  133.3 4.0 convolution_add_fusion.1
  137.3 1.2 convolution_add_fusion.7
  139.2 1.2 pad_add_fusion
  140.4 1.5 fusion.13
  142.6 1.5 convolution_bitcast_fusion.3
  145.7 11.3 %pad.33 = f32[2,8,4,64,64]{4,3,2,1,0:T(8,128)} pad(f32[2,8,2,64,64]{4,3,2,1,0:T(8,128)S(1)} %copy-done.30, f32[]{:T(128)} %constant.27.clone.1), padding=0_0_0x0_0_0x1_0_1x0_0_0x0_0_0 | pad | bytes 1572868 | tf_op jit(solution)/shard_map/pad | solution.py:212
  157.1 11.2 %pad.32 = f32[2,8,4,64,64]{4,3,2,1,0:T(8,128)} pad(f32[2,8,2,64,64]{4,3,2,1,0:T(8,128)S(1)} %pad_maximum_fusion.1, f32[]{:T(128)} %constant.27.clone.1), padding=0_0_0x0_0_0x0_1_1x0_0_0x0_0_0 | pad | bytes 1572868 | tf_op jit(solution)/shard_map/pad | solution.py:212
  168.3 11.2 %pad.28 = f32[2,8,4,64,64]{4,3,2,1,0:T(8,128)} pad(f32[2,8,2,64,64]{4,3,2,1,0:T(8,128)S(1)} %pad_maximum_fusion, f32[]{:T(128)} %constant.27.clone.1), padding=0_0_0x0_0_0x0_1_1x0_0_0x0_0_0 | pad | bytes 1572868 | tf_op jit(solution)/shard_map/pad | solution.py:212
  179.6 16.7 %pad.29 = f32[2,8,4,64,64]{4,3,2,1,0:T(8,128)} pad(f32[2,8,2,64,64]{4,3,2,1,0:T(8,128)} %pad_add_fusion.1, f32[]{:T(128)} %constant.27.clone.1), padding=0_0_0x0_0_0x1_0_1x0_0_0x0_0_0 | pad | bytes 1572868 | tf_op jit(solution)/shard_map/pad | solution.py:212
  196.3 2.2 add_convert_fusion
  198.5 10.7 %all-gather.6 = bf16[4,8,1,64,64]{4,3,2,1,0:T(8,128)(2,1)S(1)} all-gather(bf16[1,8,1,64,64]{4,3,2,1,0:T(8,128)(2,1)S(1)} %get-tuple-element.24), channel_id=8, replica_groups=mesh['sp_0'=8,'sp_1'=4,'fs'=4,'tp'=2] {'sp_1'}, dimensions={0}, use_global_device_ids=true | all-gather | bytes 327680 | tf_op jit(solution)/shard_map/all_gather | solution.py:33
  209.2 1.9 fusion.200
  211.1 11.9 %all-gather.4 = bf16[4,8,1,64,64]{4,3,2,1,0:T(8,128)(2,1)S(1)} all-gather(bf16[1,8,1,64,64]{4,3,2,1,0:T(8,128)(2,1)S(1)} %get-tuple-element.22), channel_id=6, replica_groups=mesh['sp_0'=8,'sp_1'=4,'fs'=4,'tp'=2] {'sp_1'}, dimensions={0}, use_global_device_ids=true | all-gather | bytes 327680 | tf_op jit(solution)/shard_map/all_gather | solution.py:33
  225.7 22.8 %all-gather.7 = bf16[64,64,64]{2,1,0:T(8,128)(2,1)S(1)} all-gather(bf16[8,64,64]{2,1,0:T(8,128)(2,1)S(1)} %get-tuple-element.46), channel_id=9, replica_groups=mesh['sp_0'=8,'sp_1'=4,'fs'=4,'tp'=2] {'sp_0'}, dimensions={0}, use_global_device_ids=true | all-gather | bytes 589824 | tf_op jit(solution)/shard_map/all_gather | solution.py:33
  249.3 22.2 %all-gather.5 = bf16[64,64,64]{2,1,0:T(8,128)(2,1)S(1)} all-gather(bf16[8,64,64]{2,1,0:T(8,128)(2,1)S(1)} %get-tuple-element.48), channel_id=7, replica_groups=mesh['sp_0'=8,'sp_1'=4,'fs'=4,'tp'=2] {'sp_0'}, dimensions={0}, use_global_device_ids=true | all-gather | bytes 589824 | tf_op jit(solution)/shard_map/all_gather | solution.py:33
  273.1 10.5 %all-gather.2 = bf16[4,8,1,64,64]{4,3,2,1,0:T(8,128)(2,1)S(1)} all-gather(bf16[1,8,1,64,64]{4,3,2,1,0:T(8,128)(2,1)S(1)} %get-tuple-element.23), channel_id=4, replica_groups=mesh['sp_0'=8,'sp_1'=4,'fs'=4,'tp'=2] {'sp_1'}, dimensions={0}, use_global_device_ids=true | all-gather | bytes 327680 | tf_op jit(solution)/shard_map/all_gather | solution.py:33
  283.6 10.3 %all-gather = bf16[4,8,1,64,64]{4,3,2,1,0:T(8,128)(2,1)S(1)} all-gather(bf16[1,8,1,64,64]{4,3,2,1,0:T(8,128)(2,1)S(1)} %get-tuple-element.21), channel_id=2, replica_groups=mesh['sp_0'=8,'sp_1'=4,'fs'=4,'tp'=2] {'sp_1'}, dimensions={0}, use_global_device_ids=true | all-gather | bytes 327680 | tf_op jit(solution)/shard_map/all_gather | solution.py:33
  295.9 20.4 %all-gather.3 = bf16[64,64,64]{2,1,0:T(8,128)(2,1)S(1)} all-gather(bf16[8,64,64]{2,1,0:T(8,128)(2,1)S(1)} %get-tuple-element.50), channel_id=5, replica_groups=mesh['sp_0'=8,'sp_1'=4,'fs'=4,'tp'=2] {'sp_0'}, dimensions={0}, use_global_device_ids=true | all-gather | bytes 589824 | tf_op jit(solution)/shard_map/all_gather | solution.py:33
  317.2 21.5 %all-gather.1 = bf16[64,64,64]{2,1,0:T(8,128)(2,1)S(1)} all-gather(bf16[8,64,64]{2,1,0:T(8,128)(2,1)S(1)} %get-tuple-element.52), channel_id=3, replica_groups=mesh['sp_0'=8,'sp_1'=4,'fs'=4,'tp'=2] {'sp_0'}, dimensions={0}, use_global_device_ids=true | all-gather | bytes 589824 | tf_op jit(solution)/shard_map/all_gather | solution.py:33
  345.2 3.0 fusion.30
  348.6 2.1 fusion.14
  350.7 1.8 copy.91
  352.5 1.9 stack.75
  354.4 1.8 rev.22
  356.2 2.0 copy.92
  358.2 1.3 copy.94
  359.5 1.2 copy.93
  360.8 1.3 fusion.17
  363.4 3.1 convolution_select_fusion.3
  366.5 1.2 fusion.221
  367.7 3.1 convolution_select_fusion
  370.8 1.2 convolution_add_fusion.6
  372.1 2.0 convolution_add_fusion.8
  374.1 2.0 convolution_bitcast_fusion
  376.6 3.4 fusion.9
  382.4 2.1 fusion.214
  384.5 1.9 collective-permute-start.1
  386.4 5.5 %collective-permute-start = (bf16[8,512]{1,0:T(8,128)(2,1)S(1)}, bf16[8,512]{1,0:T(8,128)(2,1)S(1)}, u32[]{:S(2)}, u32[]{:S(2)}) collective-permute-start(bf16[8,512]{1,0:T(8,128)(2,1)S(1)} %get-tuple-element.34), channel_id=1, source_target_pairs={{0,8},{8,16},{16,24},{24,32},{32,40},{40,48},{48,56},{56,64},{64,7... | collective-permute-start | bytes 24584 | tf_op jit(solution)/shard_map/ppermute | solution.py:56
  391.9 35.5 %all_to_all.32 = bf16[2,64,512]{2,1,0:T(8,128)(2,1)S(1)} all-to-all(bf16[2,64,512]{2,1,0:T(8,128)(2,1)S(1)} %multiply_convert_fusion), channel_id=1, replica_groups=mesh['sp_0'=8,'sp_1'=4,'fs'=4,'tp'=2] {'tp'}, dimensions={0} | all-to-all | bytes 262144 | tf_op jit(solution)/shard_map/all_to_all | solution.py:278
  429.2 3.9 all_to_all.33
  433.1 3.6 fusion.222
  436.7 4.3 fusion.1
  (306 shorter events, 45.8 us)
Async XLA Ops:
  6.5 5.0 %copy-start = (bf16[2048,128]{1,0:T(8,128)(2,1)S(1)}, bf16[2048,128]{1,0:T(8,128)(2,1)}, u32[]{:S(2)}) copy-start(bf16[2048,128]{1,0:T(8,128)(2,1)} %param.24) | copy-start | bytes 1572868
  6.5 4.7 %copy-start.68 = (f32[2,512]{1,0:T(2,128)S(1)}, f32[2,512]{1,0:T(2,128)}, u32[]{:S(2)}) copy-start(f32[2,512]{1,0:T(2,128)} %param.26) | copy-start | bytes 12292
  6.5 4.7 %copy-start.67 = (bf16[2048]{0:T(1024)(128)(2,1)S(1)}, bf16[2048]{0:T(1024)(128)(2,1)}, u32[]{:S(2)}) copy-start(bf16[2048]{0:T(1024)(128)(2,1)} %param.19) | copy-start | bytes 12292
  6.5 4.7 %copy-start.5 = (bf16[1,128,2048]{2,1,0:T(8,128)(2,1)S(1)}, bf16[1,128,2048]{2,1,0:T(8,128)(2,1)}, u32[]{:S(2)}) copy-start(bf16[1,128,2048]{2,1,0:T(8,128)(2,1)} %param.18) | copy-start | bytes 1572868
  6.5 38.7 %all-gather.19.cloned.1.call-start = ((), (), s32[]{:S(2)}) async-start(), calls=%async_computation.3 | async-start | bytes 2621440 | tf_op jit(solution)/shard_map/all_gather | solution.py:150
  7.3 73.2 %all-gather.21.cloned.1.call-start = ((), (), s32[]{:S(2)}) async-start(), calls=%async_computation.4 | async-start | bytes 2621440 | tf_op jit(solution)/shard_map/all_gather | solution.py:151
  8.0 3.9 copy-start.74
  8.0 337.1 %all-gather.17.cloned.1.call-start = ((), (), s32[]{:S(2)}) async-start(), calls=%async_computation.2 | async-start | bytes 2621440 | tf_op jit(solution)/shard_map/all_gather | solution.py:149
  8.8 339.4 %all-gather.23.cloned.1.call-start = ((), (), s32[]{:S(2)}) async-start(), calls=%async_computation.5 | async-start | bytes 2621440 | tf_op jit(solution)/shard_map/all_gather | solution.py:153
  9.3 372.0 %all-gather.29.cloned.1.call-start = ((), (), s32[]{:S(2)}) async-start(), calls=%async_computation.8 | async-start | bytes 2621440 | tf_op jit(solution)/shard_map/all_gather | solution.py:154
  9.9 2.6 copy-start.65
  9.9 2.6 copy-start.66
  10.0 372.0 %all-gather.27.cloned.1.call-start = ((), (), s32[]{:S(2)}) async-start(), calls=%async_computation.7 | async-start | bytes 2621440 | tf_op jit(solution)/shard_map/all_gather | solution.py:152
  10.5 422.6 %all-gather.25.cloned.1.call-start = ((), (), s32[]{:S(2)}) async-start(), calls=%async_computation.6 | async-start | bytes 6291456 | tf_op jit(solution)/shard_map/all_gather | solution.py:282
  11.5 69.0 %copy-start.62 = (f32[128]{0:T(128)}, f32[128]{0:T(128)S(1)}, u32[]{:S(2)}) copy-start(f32[128]{0:T(128)S(1)} %add_rsqrt_fusion.2) | copy-start | bytes 1540
  15.0 1.9 copy-start.72
  93.6 4.2 copy-start.9
  93.6 13.7 %copy-start.7 = (f32[2,8,4,32,64]{4,1,2,3,0:T(8,128)}, f32[2,8,4,32,64]{4,1,2,3,0:T(8,128)S(1)}, u32[]{:S(2)}) copy-start(f32[2,8,4,32,64]{4,1,2,3,0:T(8,128)S(1)} %get-tuple-element.12) | copy-start | bytes 1572868
  93.6 28.4 %copy-start.15 = (f32[2,8,4,32,64]{4,1,2,3,0:T(8,128)}, f32[2,8,4,32,64]{4,1,2,3,0:T(8,128)S(1)}, u32[]{:S(2)}) copy-start(f32[2,8,4,32,64]{4,1,2,3,0:T(8,128)S(1)} %get-tuple-element.16) | copy-start | bytes 1572868
  114.5 17.9 %copy-start.22 = (f32[1,4,32,8,64]{4,2,1,3,0:T(8,128)}, f32[1,4,32,8,64]{4,2,1,3,0:T(8,128)S(1)}, u32[]{:S(2)}) copy-start(f32[1,4,32,8,64]{4,2,1,3,0:T(8,128)S(1)} %copy.129) | copy-start | bytes 786436
  117.8 1.8 copy-start.20
  119.6 6.7 %copy-start.11 = (f32[2,8,4,32,64]{4,3,2,1,0:T(8,128)}, f32[2,8,4,32,64]{4,3,2,1,0:T(8,128)S(1)}, u32[]{:S(2)}) copy-start(f32[2,8,4,32,64]{4,3,2,1,0:T(8,128)S(1)} %convolution_negate_fusion.1) | copy-start | bytes 1572868
  122.0 4.3 copy-start.13
  122.0 4.3 copy-start.59
  131.3 11.3 %copy-start.2 = (f32[2,8,4,64,64]{4,3,2,1,0:T(8,128)}, f32[2,8,4,64,64]{4,3,2,1,0:T(8,128)S(1)}, u32[]{:S(2)}) copy-start(f32[2,8,4,64,64]{4,3,2,1,0:T(8,128)S(1)} %multiply_add_fusion) | copy-start | bytes 3145732
  131.3 2.0 copy-start.29
  137.3 4.6 %copy-start.16 = (f32[2,8,4,64,64]{4,3,2,1,0:T(8,128)}, f32[2,8,4,64,64]{4,3,2,1,0:T(8,128)S(1)}, u32[]{:S(2)}) copy-start(f32[2,8,4,64,64]{4,3,2,1,0:T(8,128)S(1)} %convolution_add_fusion.1) | copy-start | bytes 3145732
  145.6 11.3 %slice-start.1 = ((f32[2,8,4,64,64]{4,3,2,1,0:T(8,128)}), f32[2,8,1,64,64]{4,3,2,1,0:T(8,128)S(1)}, s32[]{:S(2)}) async-start(f32[2,8,4,64,64]{4,3,2,1,0:T(8,128)} %copy-done.16), calls=%async_computation.11 | async-start | bytes 1048576 | tf_op jit(solution)/shard_map/slice | solution.py:212
  145.7 11.3 %copy-start.53 = (f32[2,8,1,64,64]{4,3,2,1,0:T(8,128)S(1)}, f32[2,8,1,64,64]{4,3,2,1,0:T(8,128)}, u32[]{:S(2)}) copy-start(f32[2,8,1,64,64]{4,3,2,1,0:T(8,128)} %fusion.13) | copy-start | bytes 786436
  157.0 11.2 %slice-start = ((f32[2,8,4,64,64]{4,3,2,1,0:T(8,128)}), f32[2,8,1,64,64]{4,3,2,1,0:T(8,128)S(1)}, s32[]{:S(2)}) async-start(f32[2,8,4,64,64]{4,3,2,1,0:T(8,128)} %copy-done.2), calls=%async_computation.10 | async-start | bytes 1048576 | tf_op jit(solution)/shard_map/slice | solution.py:212
  157.0 11.2 %copy-start.54 = (f32[2,8,1,64,64]{4,3,2,1,0:T(8,128)S(1)}, f32[2,8,1,64,64]{4,3,2,1,0:T(8,128)}, u32[]{:S(2)}) copy-start(f32[2,8,1,64,64]{4,3,2,1,0:T(8,128)} %convolution_bitcast_fusion.3) | copy-start | bytes 786436
  179.6 16.7 %copy-start.3 = (f32[2,8,4,64,64]{4,3,2,1,0:T(8,128)S(1)}, f32[2,8,4,64,64]{4,3,2,1,0:T(8,128)}, u32[]{:S(2)}) copy-start(f32[2,8,4,64,64]{4,3,2,1,0:T(8,128)} %pad.33) | copy-start | bytes 3145732
  196.3 12.9 %copy-start.18 = (f32[2,8,4,64,64]{4,3,2,1,0:T(8,128)S(1)}, f32[2,8,4,64,64]{4,3,2,1,0:T(8,128)}, u32[]{:S(2)}) copy-start(f32[2,8,4,64,64]{4,3,2,1,0:T(8,128)} %pad.28) | copy-start | bytes 3145732
  196.3 12.9 %copy-start.19 = (f32[2,8,4,64,64]{4,3,2,1,0:T(8,128)S(1)}, f32[2,8,4,64,64]{4,3,2,1,0:T(8,128)}, u32[]{:S(2)}) copy-start(f32[2,8,4,64,64]{4,3,2,1,0:T(8,128)} %pad.29) | copy-start | bytes 3145732
  224.5 24.6 %copy-start.33 = (f32[8,64,64]{2,1,0:T(8,128)}, f32[8,64,64]{2,1,0:T(8,128)S(1)}, u32[]{:S(2)}) copy-start(f32[8,64,64]{2,1,0:T(8,128)S(1)} %convolution_add_fusion.19) | copy-start | bytes 393220
  224.8 24.6 %copy-start.34 = (f32[8,64,64]{2,1,0:T(8,128)}, f32[8,64,64]{2,1,0:T(8,128)S(1)}, u32[]{:S(2)}) copy-start(f32[8,64,64]{2,1,0:T(8,128)S(1)} %convolution_add_fusion.18) | copy-start | bytes 393220
  294.4 22.3 %copy-start.45 = (f32[8,64,64]{2,1,0:T(8,128)}, f32[8,64,64]{2,1,0:T(8,128)S(1)}, u32[]{:S(2)}) copy-start(f32[8,64,64]{2,1,0:T(8,128)S(1)} %convolution_add_fusion.33) | copy-start | bytes 393220
  316.4 24.8 %copy-start.26 = (bf16[64,64,64]{2,1,0:T(8,128)(2,1)}, bf16[64,64,64]{2,1,0:T(8,128)(2,1)S(1)}, u32[]{:S(2)}) copy-start(bf16[64,64,64]{2,1,0:T(8,128)(2,1)S(1)} %all-gather.3) | copy-start | bytes 1572868
  338.7 2.5 copy-start.27
  340.1 2.1 copy-start.35
  340.4 1.8 copy-start.37
  342.6 2.5 copy-start.63
  348.2 88.5 %all-gather.31.cloned.1.call-start = ((), (), s32[]{:S(2)}) async-start(), calls=%async_computation.9 | async-start | bytes 6291456 | tf_op jit(solution)/shard_map/all_gather | solution.py:283
  358.1 2.6 copy-start.36
  358.1 2.6 copy-start.38
  358.1 2.6 copy-start.40
  358.1 2.6 copy-start.42
  358.2 2.6 copy-start.44
  358.2 2.6 copy-start.49
  358.2 2.6 copy-start.56
  358.2 4.0 copy-start.57
  359.5 3.1 copy-start.32
  359.5 3.1 copy-start.46
  359.5 3.1 copy-start.55
  360.8 2.2 copy-start.50
  363.4 3.1 copy-start.14
  367.7 3.1 copy-start.21
  367.7 3.1 copy-start.23
  372.0 2.1 copy-start.17
  374.1 2.0 copy-start.4
  381.8 10.1 %copy-start.64 = (f32[512]{0:T(512)S(1)}, f32[512]{0:T(512)}, u32[]{:S(2)}) copy-start(f32[512]{0:T(512)} %convert_element_type.431) | copy-start | bytes 6148
  384.5 43.0 %collective-permute-start.1 = (bf16[8,512]{1,0:T(8,128)(2,1)S(1)}, bf16[8,512]{1,0:T(8,128)(2,1)S(1)}, u32[]{:S(2)}, u32[]{:S(2)}) collective-permute-start(bf16[8,512]{1,0:T(8,128)(2,1)S(1)} %get-tuple-element.35), channel_id=1, source_target_pairs={{8,0},{16,8},{24,16},{32,24},{40,32},{48,40},{56,48},{64,56},{72,6... | collective-permute-start | bytes 24584 | tf_op jit(solution)/shard_map/ppermute | solution.py:58
  386.4 41.1 %collective-permute-start = (bf16[8,512]{1,0:T(8,128)(2,1)S(1)}, bf16[8,512]{1,0:T(8,128)(2,1)S(1)}, u32[]{:S(2)}, u32[]{:S(2)}) collective-permute-start(bf16[8,512]{1,0:T(8,128)(2,1)S(1)} %get-tuple-element.34), channel_id=1, source_target_pairs={{0,8},{8,16},{16,24},{24,32},{32,40},{40,48},{48,56},{56,64},{64,7... | collective-permute-start | bytes 24584 | tf_op jit(solution)/shard_map/ppermute | solution.py:56
  436.7 4.4 copy-start.1
  (24 other events, 28.0 us)
Sparse Core Ops, SparseCore 0:
  9.2 36.0 all-gather.18
  47.1 33.3 all-gather.20
  82.3 33.3 all-gather.16
  117.4 33.3 all-gather.22
  152.5 33.3 all-gather.28
  187.5 33.3 all-gather.26
  348.3 47.0 all-gather.24
  397.2 31.7 all-gather.30
where the time goes:
time: 454 us; the launch traced here: 448 us
  blocking collectives  170 us (37%)
  matrix products  97.3 us (21%)
  local copies, waits for them, and re-layouts  78.8 us (17%)
  waiting for transfers between devices  63.8 us (14%)
  between operations  15.5 us (3%)
  other arithmetic  15 us (3%)
  starting transfers between devices  8.1 us (2%)
    all_gather x8, blocking collectives, prefix_by_axis(): lax.all_gather(part.astype(kind), axis)  130 us
    dot_general x67, matrix products, contract(): return jnp.einsum(form, left, right, precision=highest)  77.8 us
    pad x4, local copies, waits for them, and re-layouts, shards(): lax.associative_scan(chain_combine, (transfer, carried), axis=2)  50.4 us
    all_to_all x1, blocking collectives, shards(): lax.all_to_all(attn_out, 'tp', split_axis=0, concat_axis=1, tiled=True)  35.5 us
    all_gather x1, waiting for transfers between devices, shards(): lax.all_gather(value_matrix, 'fs', axis=0, tiled=True)  32.9 us
    all_gather x1, waiting for transfers between devices, shards(): lax.all_gather(key_matrix, 'fs', axis=0, tiled=True)  27.2 us
    dot_general x6, matrix products, project(): jnp.dot(left, weight, preferred_element_type=jnp.float32)  10 us
    rev x12, local copies, waits for them, and re-layouts, both_ways(): stacked = jnp.stack([forward, jnp.flip(backward, axis=0)], axis=0)  9.63 us
  transfers between devices with their start and end apart: 10, of which 2 were waited for; matrix products, arithmetic and copies ran while one was open for 40% of the time, Pallas kernels for 0%

commit v1 on v0

--- a/solution.py
+++ b/solution.py
@@ -148,7 +148,9 @@
     recept_full, key_full, value_full, pool_full, attn_full, pool_back = (
         lax.all_gather(receptance_matrix, "fs", axis=0, tiled=True),
         lax.all_gather(key_matrix, "fs", axis=0, tiled=True),
-        lax.all_gather(value_matrix, "fs", axis=0, tiled=True),
+        jnp.concatenate(
+            lax.all_to_all(jnp.stack([value_matrix] * lax.axis_size("fs")), "fs", 0, 0), axis=0
+        ),
         lax.all_gather(pooling_input_weight, "fs", axis=0, tiled=True),
         lax.all_gather(attention_output_matrix, "fs", axis=0, tiled=True),
         lax.all_gather(pooling_output_matrix, "fs", axis=0, tiled=True),

time: 454 us -> 429 us (0.945)
  waiting for transfers between devices: 63.8 us -> 32.8 us
  matrix products: 97.3 us -> 90.9 us
  blocking collectives: 170 us -> 175 us
    all_gather x1 -> x0, waiting for transfers between devices: 32.9 us -> none  [shards(): lax.all_gather(value_matrix, 'fs', axis=0, tiled=True)]
    all_to_all x0 -> x1, waiting for transfers between devices: none -> 28.8 us  [shards(): lax.all_to_all(jnp.stack([value_matrix] * lax.axis_size('fs')), 'fs', 0, 0)]
    all_gather x1, waiting for transfers between devices: 27.2 us -> 0.71 us  [shards(): lax.all_gather(key_matrix, 'fs', axis=0, tiled=True)]
    dot_general x67, matrix products: 77.8 us -> 71.4 us  [contract(): return jnp.einsum(form, left, right, precision=highest)]
    all_to_all x0 -> x1, starting transfers between devices: none -> 4.59 us  [shards(): lax.all_to_all(jnp.stack([value_matrix] * lax.axis_size('fs')), 'fs', 0, 0)]
  transfers between devices with their start and end apart: 10 -> 10, of which waited for: 2 -> 2; matrix products, arithmetic and copies ran while one was open for 40% -> 42% of each run, Pallas kernels for 0% -> 0%
where the time goes in v1:
time: 429 us; the launch traced here: 423 us
  blocking collectives  175 us (41%)
  matrix products  90.9 us (21%)
  local copies, waits for them, and re-layouts  81.4 us (19%)
  waiting for transfers between devices  32.8 us (8%)
  between operations  15.6 us (4%)
  other arithmetic  15.1 us (4%)
  starting transfers between devices  12.6 us (3%)
    all_gather x8, blocking collectives, prefix_by_axis(): lax.all_gather(part.astype(kind), axis)  131 us
    dot_general x67, matrix products, contract(): return jnp.einsum(form, left, right, precision=highest)  71.4 us
    pad x4, local copies, waits for them, and re-layouts, shards(): lax.associative_scan(chain_combine, (transfer, carried), axis=2)  50.4 us
    all_to_all x1, blocking collectives, shards(): lax.all_to_all(attn_out, 'tp', split_axis=0, concat_axis=1, tiled=True)  39.9 us
    all_to_all x1, waiting for transfers between devices, shards(): lax.all_to_all(jnp.stack([value_matrix] * lax.axis_size('fs')), 'fs', 0, 0)  28.8 us
    rev x12, local copies, waits for them, and re-layouts, both_ways(): stacked = jnp.stack([forward, jnp.flip(backward, axis=0)], axis=0)  10.5 us
    dot_general x6, matrix products, project(): jnp.dot(left, weight, preferred_element_type=jnp.float32)  10 us
  transfers between devices with their start and end apart: 10, of which 2 were waited for; matrix products, arithmetic and copies ran while one was open for 42% of the time, Pallas kernels for 0%

profile of v1, /device:TPU:7, one launch (start us, length us, event | category | flops | bytes accessed | tf_op | source)
XLA Modules:
  0.0 423.5 jit_solution(6375265814943166524)
XLA Ops:
  9.3 1.6 stack.93
  10.9 4.6 %all-to-all-start = ((bf16[4,512,512]{2,1,0:T(8,128)(2,1)}), bf16[4,512,512]{2,1,0:T(8,128)(2,1)}, u32[]{:S(2)}, u32[]{:S(2)}) async-start(bf16[4,512,512]{2,1,0:T(8,128)(2,1)} %stack.93), calls=%async_computation | async-start | bytes 4194304 | tf_op jit(solution)/shard_map/all_to_all | solution.py:152
  24.8 28.8 %all-to-all-done = bf16[4,512,512]{2,1,0:T(8,128)(2,1)} async-done(((bf16[4,512,512]{2,1,0:T(8,128)(2,1)}), bf16[4,512,512]{2,1,0:T(8,128)(2,1)}, u32[]{:S(2)}, u32[]{:S(2)}) %all-to-all-start) | async-done | bytes 2097184 | tf_op jit(solution)/shard_map/all_to_all | solution.py:152
  53.6 2.1 fusion.30
  57.1 1.3 copy.129
  59.2 2.1 fusion.31
  63.0 1.7 fusion.208
  68.8 2.0 copy.123
  70.7 1.5 copy_multiply_fusion.2
  73.2 3.0 convolution_select_fusion.2
  77.4 1.2 fusion.223
  78.6 1.3 convolution_add_fusion.5
  79.9 1.2 fusion.224
  81.1 1.4 convolution_add_fusion.4
  82.5 1.2 fusion.225
  83.7 1.2 convolution_add_fusion.3
  84.9 3.0 convolution_select_fusion.1
  88.0 1.2 convolution_add_fusion.2
  89.1 1.7 convolution_negate_fusion.1
  90.9 1.2 fusion.65
  93.3 4.2 fusion.50
  97.5 3.7 multiply_add_fusion
  101.3 1.2 fusion.45
  103.2 4.0 convolution_add_fusion.1
  107.3 1.2 convolution_add_fusion.7
  110.4 1.5 fusion.15
  112.5 1.5 convolution_bitcast_fusion.3
  115.6 11.3 %pad.33 = f32[2,8,4,64,64]{4,3,2,1,0:T(8,128)} pad(f32[2,8,2,64,64]{4,3,2,1,0:T(8,128)S(1)} %copy-done.29, f32[]{:T(128)} %constant.27.clone.1), padding=0_0_0x0_0_0x1_0_1x0_0_0x0_0_0 | pad | bytes 1572868 | tf_op jit(solution)/shard_map/pad | solution.py:214
  127.0 11.2 %pad.32 = f32[2,8,4,64,64]{4,3,2,1,0:T(8,128)} pad(f32[2,8,2,64,64]{4,3,2,1,0:T(8,128)S(1)} %pad_maximum_fusion.1, f32[]{:T(128)} %constant.27.clone.1), padding=0_0_0x0_0_0x0_1_1x0_0_0x0_0_0 | pad | bytes 1572868 | tf_op jit(solution)/shard_map/pad | solution.py:214
  138.3 11.2 %pad.28 = f32[2,8,4,64,64]{4,3,2,1,0:T(8,128)} pad(f32[2,8,2,64,64]{4,3,2,1,0:T(8,128)S(1)} %pad_maximum_fusion, f32[]{:T(128)} %constant.27.clone.1), padding=0_0_0x0_0_0x0_1_1x0_0_0x0_0_0 | pad | bytes 1572868 | tf_op jit(solution)/shard_map/pad | solution.py:214
  149.6 16.7 %pad.29 = f32[2,8,4,64,64]{4,3,2,1,0:T(8,128)} pad(f32[2,8,2,64,64]{4,3,2,1,0:T(8,128)} %pad_add_fusion.1, f32[]{:T(128)} %constant.27.clone.1), padding=0_0_0x0_0_0x1_0_1x0_0_0x0_0_0 | pad | bytes 1572868 | tf_op jit(solution)/shard_map/pad | solution.py:214
  166.3 2.2 add_convert_fusion
  168.5 9.9 %all-gather.6 = bf16[4,8,1,64,64]{4,3,2,1,0:T(8,128)(2,1)S(1)} all-gather(bf16[1,8,1,64,64]{4,3,2,1,0:T(8,128)(2,1)S(1)} %get-tuple-element.24), channel_id=8, replica_groups=mesh['sp_0'=8,'sp_1'=4,'fs'=4,'tp'=2] {'sp_1'}, dimensions={0}, use_global_device_ids=true | all-gather | bytes 327680 | tf_op jit(solution)/shard_map/all_gather | solution.py:33
  178.4 1.9 fusion.207
  180.3 11.1 %all-gather.4 = bf16[4,8,1,64,64]{4,3,2,1,0:T(8,128)(2,1)S(1)} all-gather(bf16[1,8,1,64,64]{4,3,2,1,0:T(8,128)(2,1)S(1)} %get-tuple-element.22), channel_id=6, replica_groups=mesh['sp_0'=8,'sp_1'=4,'fs'=4,'tp'=2] {'sp_1'}, dimensions={0}, use_global_device_ids=true | all-gather | bytes 327680 | tf_op jit(solution)/shard_map/all_gather | solution.py:33
  194.2 26.6 %all-gather.7 = bf16[64,64,64]{2,1,0:T(8,128)(2,1)S(1)} all-gather(bf16[8,64,64]{2,1,0:T(8,128)(2,1)S(1)} %get-tuple-element.46), channel_id=9, replica_groups=mesh['sp_0'=8,'sp_1'=4,'fs'=4,'tp'=2] {'sp_0'}, dimensions={0}, use_global_device_ids=true | all-gather | bytes 589824 | tf_op jit(solution)/shard_map/all_gather | solution.py:33
  221.6 21.2 %all-gather.5 = bf16[64,64,64]{2,1,0:T(8,128)(2,1)S(1)} all-gather(bf16[8,64,64]{2,1,0:T(8,128)(2,1)S(1)} %get-tuple-element.48), channel_id=7, replica_groups=mesh['sp_0'=8,'sp_1'=4,'fs'=4,'tp'=2] {'sp_0'}, dimensions={0}, use_global_device_ids=true | all-gather | bytes 589824 | tf_op jit(solution)/shard_map/all_gather | solution.py:33
  244.4 10.5 %all-gather.2 = bf16[4,8,1,64,64]{4,3,2,1,0:T(8,128)(2,1)S(1)} all-gather(bf16[1,8,1,64,64]{4,3,2,1,0:T(8,128)(2,1)S(1)} %get-tuple-element.23), channel_id=4, replica_groups=mesh['sp_0'=8,'sp_1'=4,'fs'=4,'tp'=2] {'sp_1'}, dimensions={0}, use_global_device_ids=true | all-gather | bytes 327680 | tf_op jit(solution)/shard_map/all_gather | solution.py:33
  254.9 9.9 %all-gather = bf16[4,8,1,64,64]{4,3,2,1,0:T(8,128)(2,1)S(1)} all-gather(bf16[1,8,1,64,64]{4,3,2,1,0:T(8,128)(2,1)S(1)} %get-tuple-element.21), channel_id=2, replica_groups=mesh['sp_0'=8,'sp_1'=4,'fs'=4,'tp'=2] {'sp_1'}, dimensions={0}, use_global_device_ids=true | all-gather | bytes 327680 | tf_op jit(solution)/shard_map/all_gather | solution.py:33
  266.8 20.6 %all-gather.3 = bf16[64,64,64]{2,1,0:T(8,128)(2,1)S(1)} all-gather(bf16[8,64,64]{2,1,0:T(8,128)(2,1)S(1)} %get-tuple-element.50), channel_id=5, replica_groups=mesh['sp_0'=8,'sp_1'=4,'fs'=4,'tp'=2] {'sp_0'}, dimensions={0}, use_global_device_ids=true | all-gather | bytes 589824 | tf_op jit(solution)/shard_map/all_gather | solution.py:33
  288.3 21.5 %all-gather.1 = bf16[64,64,64]{2,1,0:T(8,128)(2,1)S(1)} all-gather(bf16[8,64,64]{2,1,0:T(8,128)(2,1)S(1)} %get-tuple-element.52), channel_id=3, replica_groups=mesh['sp_0'=8,'sp_1'=4,'fs'=4,'tp'=2] {'sp_0'}, dimensions={0}, use_global_device_ids=true | all-gather | bytes 589824 | tf_op jit(solution)/shard_map/all_gather | solution.py:33
  316.2 3.0 fusion.32
  319.6 2.1 fusion.16
  321.7 1.8 copy.91
  323.5 1.9 stack.82
  325.4 1.8 rev.22
  327.2 2.0 copy.92
  329.2 1.3 copy.94
  330.5 1.2 copy.93
  331.8 1.3 fusion.19
  334.4 3.1 convolution_select_fusion.3
  337.5 1.2 fusion.228
  338.7 3.1 convolution_select_fusion
  341.8 1.2 convolution_add_fusion.6
  343.1 2.0 convolution_add_fusion.8
  345.1 2.0 convolution_bitcast_fusion
  347.6 3.4 fusion.9
  353.4 2.1 fusion.221
  355.5 1.9 collective-permute-start.1
  357.4 5.5 %collective-permute-start = (bf16[8,512]{1,0:T(8,128)(2,1)S(1)}, bf16[8,512]{1,0:T(8,128)(2,1)S(1)}, u32[]{:S(2)}, u32[]{:S(2)}) collective-permute-start(bf16[8,512]{1,0:T(8,128)(2,1)S(1)} %get-tuple-element.34), channel_id=1, source_target_pairs={{0,8},{8,16},{16,24},{24,32},{32,40},{40,48},{48,56},{56,64},{64,7... | collective-permute-start | bytes 24584 | tf_op jit(solution)/shard_map/ppermute | solution.py:56
  363.0 39.9 %all_to_all.37 = bf16[2,64,512]{2,1,0:T(8,128)(2,1)S(1)} all-to-all(bf16[2,64,512]{2,1,0:T(8,128)(2,1)S(1)} %multiply_convert_fusion), channel_id=1, replica_groups=mesh['sp_0'=8,'sp_1'=4,'fs'=4,'tp'=2] {'tp'}, dimensions={0} | all-to-all | bytes 262144 | tf_op jit(solution)/shard_map/all_to_all | solution.py:280
  404.6 3.9 all_to_all.38
  408.5 3.6 fusion.229
  412.1 4.3 %fusion.1 = bf16[1,64,2048]{2,1,0:T(8,128)(2,1)} fusion(f32[64,2048]{1,0:T(8,128)S(1)} %fusion.229, bf16[64,1024]{1,0:T(8,128)(2,1)S(1)} %bitcast.409, bf16[2048,1024]{1,0:T(8,128)(2,1)} %all-gather.28.cloned.1.call-done), kind=kOutput, calls=%fused_computation.2 | convolution fusion | flops 268697600 | bytes 5111808 | tf_op jit(solution)/shard_map/dot_general | solution.py:78
  (308 shorter events, 48.2 us)
Async XLA Ops:
  6.5 9.9 %copy-start = (bf16[2048,128]{1,0:T(8,128)(2,1)S(1)}, bf16[2048,128]{1,0:T(8,128)(2,1)}, u32[]{:S(2)}) copy-start(bf16[2048,128]{1,0:T(8,128)(2,1)} %param.24) | copy-start | bytes 1572868
  6.5 2.8 copy-start.58
  6.5 52.6 %all-gather.18.cloned.1.call-start = ((), (), s32[]{:S(2)}) async-start(), calls=%async_computation.4 | async-start | bytes 2621440 | tf_op jit(solution)/shard_map/all_gather | solution.py:150
  7.3 308.9 %all-gather.16.cloned.1.call-start = ((), (), s32[]{:S(2)}) async-start(), calls=%async_computation.3 | async-start | bytes 2621440 | tf_op jit(solution)/shard_map/all_gather | solution.py:149
  8.0 311.1 %all-gather.20.cloned.1.call-start = ((), (), s32[]{:S(2)}) async-start(), calls=%async_computation.5 | async-start | bytes 2621440 | tf_op jit(solution)/shard_map/all_gather | solution.py:155
  8.7 343.6 %all-gather.26.cloned.1.call-start = ((), (), s32[]{:S(2)}) async-start(), calls=%async_computation.8 | async-start | bytes 2621440 | tf_op jit(solution)/shard_map/all_gather | solution.py:156
  10.9 5.3 %copy-start.69 = (f32[2,512]{1,0:T(2,128)S(1)}, f32[2,512]{1,0:T(2,128)}, u32[]{:S(2)}) copy-start(f32[2,512]{1,0:T(2,128)} %param.26) | copy-start | bytes 12292
  10.9 5.4 %copy-start.68 = (bf16[2048]{0:T(1024)(128)(2,1)S(1)}, bf16[2048]{0:T(1024)(128)(2,1)}, u32[]{:S(2)}) copy-start(bf16[2048]{0:T(1024)(128)(2,1)} %param.19) | copy-start | bytes 12292
  10.9 5.4 %copy-start.5 = (bf16[1,128,2048]{2,1,0:T(8,128)(2,1)S(1)}, bf16[1,128,2048]{2,1,0:T(8,128)(2,1)}, u32[]{:S(2)}) copy-start(bf16[1,128,2048]{2,1,0:T(8,128)(2,1)} %param.18) | copy-start | bytes 1572868
  10.9 42.7 %all-to-all-start = ((bf16[4,512,512]{2,1,0:T(8,128)(2,1)}), bf16[4,512,512]{2,1,0:T(8,128)(2,1)}, u32[]{:S(2)}, u32[]{:S(2)}) async-start(bf16[4,512,512]{2,1,0:T(8,128)(2,1)} %stack.93), calls=%async_computation | async-start | bytes 4194304 | tf_op jit(solution)/shard_map/all_to_all | solution.py:152
  15.5 2.0 copy-start.66
  15.5 2.0 copy-start.67
  15.5 337.5 %all-gather.24.cloned.1.call-start = ((), (), s32[]{:S(2)}) async-start(), calls=%async_computation.7 | async-start | bytes 2621440 | tf_op jit(solution)/shard_map/all_gather | solution.py:154
  16.1 392.3 %all-gather.22.cloned.1.call-start = ((), (), s32[]{:S(2)}) async-start(), calls=%async_computation.6 | async-start | bytes 6291456 | tf_op jit(solution)/shard_map/all_gather | solution.py:284
  16.5 42.7 %copy-start.63 = (f32[128]{0:T(128)}, f32[128]{0:T(128)S(1)}, u32[]{:S(2)}) copy-start(f32[128]{0:T(128)S(1)} %add_rsqrt_fusion.2) | copy-start | bytes 1540
  20.7 2.2 copy-start.73
  21.9 33.8 %copy-start.25 = (f32[1,4,32,8,64]{4,3,1,2,0:T(8,128)}, f32[1,4,32,8,64]{4,3,1,2,0:T(8,128)S(1)}, u32[]{:S(2)}) copy-start(f32[1,4,32,8,64]{4,3,1,2,0:T(8,128)S(1)} %fusion.77) | copy-start | bytes 786436
  57.1 33.8 %copy-start.19 = (f32[128,8,64]{2,0,1:T(8,128)}, f32[128,8,64]{2,0,1:T(8,128)S(1)}, u32[]{:S(2)}) copy-start(f32[128,8,64]{2,0,1:T(8,128)S(1)} %copy.128) | copy-start | bytes 786436
  58.5 32.4 %copy-start.22 = (f32[1,4,32,8,64]{4,2,1,3,0:T(8,128)}, f32[1,4,32,8,64]{4,2,1,3,0:T(8,128)S(1)}, u32[]{:S(2)}) copy-start(f32[1,4,32,8,64]{4,2,1,3,0:T(8,128)S(1)} %copy.129) | copy-start | bytes 786436
  67.9 4.4 %copy-start.26 = (f32[1,4,32,8,64]{4,3,1,2,0:T(8,128)S(1)}, f32[1,4,32,8,64]{4,3,1,2,0:T(8,128)}, u32[]{:S(2)}) copy-start(f32[1,4,32,8,64]{4,3,1,2,0:T(8,128)} %copy-done.25) | copy-start | bytes 786436
  73.2 4.2 copy-start.9
  73.2 11.7 %copy-start.7 = (f32[2,8,4,32,64]{4,1,2,3,0:T(8,128)}, f32[2,8,4,32,64]{4,1,2,3,0:T(8,128)S(1)}, u32[]{:S(2)}) copy-start(f32[2,8,4,32,64]{4,1,2,3,0:T(8,128)S(1)} %get-tuple-element.12) | copy-start | bytes 1572868
  90.9 6.6 %copy-start.11 = (f32[2,8,4,32,64]{4,3,2,1,0:T(8,128)}, f32[2,8,4,32,64]{4,3,2,1,0:T(8,128)S(1)}, u32[]{:S(2)}) copy-start(f32[2,8,4,32,64]{4,3,2,1,0:T(8,128)S(1)} %convolution_negate_fusion.1) | copy-start | bytes 1572868
  93.3 4.2 %copy-start.13 = (f32[2,8,4,32,64]{4,3,2,1,0:T(8,128)}, f32[2,8,4,32,64]{4,3,2,1,0:T(8,128)S(1)}, u32[]{:S(2)}) copy-start(f32[2,8,4,32,64]{4,3,2,1,0:T(8,128)S(1)} %convolution_negate_fusion) | copy-start | bytes 1572868
  93.3 4.2 %copy-start.60 = (f32[2,8,4,64]{3,2,1,0:T(4,128)S(1)}, f32[2,8,4,64]{3,2,1,0:T(4,128)}, u32[]{:S(2)}) copy-start(f32[2,8,4,64]{3,2,1,0:T(4,128)} %copy.115) | copy-start | bytes 49156
  101.3 11.3 %copy-start.2 = (f32[2,8,4,64,64]{4,3,2,1,0:T(8,128)}, f32[2,8,4,64,64]{4,3,2,1,0:T(8,128)S(1)}, u32[]{:S(2)}) copy-start(f32[2,8,4,64,64]{4,3,2,1,0:T(8,128)S(1)} %multiply_add_fusion) | copy-start | bytes 3145732
  101.3 1.9 copy-start.23
  107.3 4.6 %copy-start.15 = (f32[2,8,4,64,64]{4,3,2,1,0:T(8,128)}, f32[2,8,4,64,64]{4,3,2,1,0:T(8,128)S(1)}, u32[]{:S(2)}) copy-start(f32[2,8,4,64,64]{4,3,2,1,0:T(8,128)S(1)} %convolution_add_fusion.1) | copy-start | bytes 3145732
  115.6 11.3 %slice-start.1 = ((f32[2,8,4,64,64]{4,3,2,1,0:T(8,128)}), f32[2,8,1,64,64]{4,3,2,1,0:T(8,128)S(1)}, s32[]{:S(2)}) async-start(f32[2,8,4,64,64]{4,3,2,1,0:T(8,128)} %copy-done.15), calls=%async_computation.11 | async-start | bytes 1048576 | tf_op jit(solution)/shard_map/slice | solution.py:214
  115.6 11.3 %copy-start.53 = (f32[2,8,1,64,64]{4,3,2,1,0:T(8,128)S(1)}, f32[2,8,1,64,64]{4,3,2,1,0:T(8,128)}, u32[]{:S(2)}) copy-start(f32[2,8,1,64,64]{4,3,2,1,0:T(8,128)} %fusion.15) | copy-start | bytes 786436
  127.0 11.2 %slice-start = ((f32[2,8,4,64,64]{4,3,2,1,0:T(8,128)}), f32[2,8,1,64,64]{4,3,2,1,0:T(8,128)S(1)}, s32[]{:S(2)}) async-start(f32[2,8,4,64,64]{4,3,2,1,0:T(8,128)} %copy-done.2), calls=%async_computation.10 | async-start | bytes 1048576 | tf_op jit(solution)/shard_map/slice | solution.py:214
  127.0 11.2 %copy-start.54 = (f32[2,8,1,64,64]{4,3,2,1,0:T(8,128)S(1)}, f32[2,8,1,64,64]{4,3,2,1,0:T(8,128)}, u32[]{:S(2)}) copy-start(f32[2,8,1,64,64]{4,3,2,1,0:T(8,128)} %convolution_bitcast_fusion.3) | copy-start | bytes 786436
  149.6 16.7 %copy-start.3 = (f32[2,8,4,64,64]{4,3,2,1,0:T(8,128)S(1)}, f32[2,8,4,64,64]{4,3,2,1,0:T(8,128)}, u32[]{:S(2)}) copy-start(f32[2,8,4,64,64]{4,3,2,1,0:T(8,128)} %pad.33) | copy-start | bytes 3145732
  166.3 12.1 %copy-start.17 = (f32[2,8,4,64,64]{4,3,2,1,0:T(8,128)S(1)}, f32[2,8,4,64,64]{4,3,2,1,0:T(8,128)}, u32[]{:S(2)}) copy-start(f32[2,8,4,64,64]{4,3,2,1,0:T(8,128)} %pad.28) | copy-start | bytes 3145732
  166.3 12.1 %copy-start.18 = (f32[2,8,4,64,64]{4,3,2,1,0:T(8,128)S(1)}, f32[2,8,4,64,64]{4,3,2,1,0:T(8,128)}, u32[]{:S(2)}) copy-start(f32[2,8,4,64,64]{4,3,2,1,0:T(8,128)} %pad.29) | copy-start | bytes 3145732
  192.9 28.4 %copy-start.32 = (f32[8,64,64]{2,1,0:T(8,128)}, f32[8,64,64]{2,1,0:T(8,128)S(1)}, u32[]{:S(2)}) copy-start(f32[8,64,64]{2,1,0:T(8,128)S(1)} %convolution_add_fusion.19) | copy-start | bytes 393220
  193.2 28.4 %copy-start.33 = (f32[8,64,64]{2,1,0:T(8,128)}, f32[8,64,64]{2,1,0:T(8,128)S(1)}, u32[]{:S(2)}) copy-start(f32[8,64,64]{2,1,0:T(8,128)S(1)} %convolution_add_fusion.18) | copy-start | bytes 393220
  265.3 22.4 %copy-start.44 = (f32[8,64,64]{2,1,0:T(8,128)}, f32[8,64,64]{2,1,0:T(8,128)S(1)}, u32[]{:S(2)}) copy-start(f32[8,64,64]{2,1,0:T(8,128)S(1)} %convolution_add_fusion.33) | copy-start | bytes 393220
  287.5 24.8 %copy-start.27 = (bf16[64,64,64]{2,1,0:T(8,128)(2,1)}, bf16[64,64,64]{2,1,0:T(8,128)(2,1)S(1)}, u32[]{:S(2)}) copy-start(bf16[64,64,64]{2,1,0:T(8,128)(2,1)S(1)} %all-gather.3) | copy-start | bytes 1572868
  309.8 2.5 copy-start.28
  311.1 2.1 copy-start.34
  313.7 2.5 copy-start.64
  319.2 92.9 %all-gather.28.cloned.1.call-start = ((), (), s32[]{:S(2)}) async-start(), calls=%async_computation.9 | async-start | bytes 6291456 | tf_op jit(solution)/shard_map/all_gather | solution.py:285
  329.2 2.6 copy-start.35
  329.2 2.6 copy-start.37
  329.2 2.6 copy-start.39
  329.2 2.6 copy-start.41
  329.2 2.6 copy-start.43
  329.2 2.6 copy-start.48
  329.2 2.6 copy-start.56
  329.2 4.0 copy-start.57
  330.5 3.1 copy-start.31
  330.5 3.1 copy-start.45
  330.5 3.1 copy-start.55
  331.8 2.2 copy-start.49
  334.4 3.1 copy-start.14
  338.7 3.1 copy-start.21
  338.7 3.1 copy-start.24
  343.1 2.1 copy-start.16
  345.1 2.0 copy-start.4
  352.8 10.1 %copy-start.65 = (f32[512]{0:T(512)S(1)}, f32[512]{0:T(512)}, u32[]{:S(2)}) copy-start(f32[512]{0:T(512)} %convert_element_type.442) | copy-start | bytes 6148
  355.5 47.3 %collective-permute-start.1 = (bf16[8,512]{1,0:T(8,128)(2,1)S(1)}, bf16[8,512]{1,0:T(8,128)(2,1)S(1)}, u32[]{:S(2)}, u32[]{:S(2)}) collective-permute-start(bf16[8,512]{1,0:T(8,128)(2,1)S(1)} %get-tuple-element.35), channel_id=1, source_target_pairs={{8,0},{16,8},{24,16},{32,24},{40,32},{48,40},{56,48},{64,56},{72,6... | collective-permute-start | bytes 24584 | tf_op jit(solution)/shard_map/ppermute | solution.py:58
  357.4 45.4 %collective-permute-start = (bf16[8,512]{1,0:T(8,128)(2,1)S(1)}, bf16[8,512]{1,0:T(8,128)(2,1)S(1)}, u32[]{:S(2)}, u32[]{:S(2)}) collective-permute-start(bf16[8,512]{1,0:T(8,128)(2,1)S(1)} %get-tuple-element.34), channel_id=1, source_target_pairs={{0,8},{8,16},{16,24},{24,32},{32,40},{40,48},{48,56},{56,64},{64,7... | collective-permute-start | bytes 24584 | tf_op jit(solution)/shard_map/ppermute | solution.py:56
  412.1 4.4 %copy-start.1 = (bf16[2048,128]{1,0:T(8,128)(2,1)S(1)}, bf16[2048,128]{1,0:T(8,128)(2,1)}, u32[]{:S(2)}) copy-start(bf16[2048,128]{1,0:T(8,128)(2,1)} %param.24) | copy-start | bytes 1572868
  (25 other events, 31.4 us)
Sparse Core Ops, SparseCore 0:
  9.1 49.9 all-gather.17
  61.0 34.2 all-gather.15
  97.1 33.3 all-gather.19
  132.1 33.3 all-gather.25
  167.2 33.3 all-gather.23
  319.3 51.1 all-gather.21
  372.3 31.7 all-gather.27
